TPU v7x, 32 devices: a whole 2x2x4 slice. The times are simulated.
32 devices in a mesh: grp: 2 (over y), sp: 4 (over z), dp: 4 (over x, core).
Axes of the slice: x: 2, y: 2, z: 4, core: 2. Of those that a mesh axis runs over, the one named last changes fastest.
Arguments:
- activations: bfloat16 [8, 2048, 2048], P(('grp', 'dp'), 'sp'), parts along dimension 0, may hold values from -6 to 6
- value_weight: bfloat16 [2048, 1024], P('sp', 'dp'), may hold values from -0.125 to 0.125
- gate_weight: bfloat16 [2048, 1024], P('sp', 'dp'), may hold values from -0.125 to 0.125
- conv_taps: float32 [31, 1024], replicated, may hold values from -4 to 4
- conv_bias: float32 [1024], replicated, may hold values from -3 to 3
- norm_gain: float32 [1024], replicated, may hold values from 0.1 to 1.9
- norm_bias: float32 [1024], replicated, may hold values from -3 to 3
- out_weight: bfloat16 [1024, 2048], P('sp', 'dp'), may hold values from -0.1875 to 0.1875
Outputs:
- mixed_out: bfloat16 [8, 2048, 2048], P(('grp', 'dp'), 'sp'), parts along dimension 0
There are 2 independent parts, one for each index of `grp`. A program takes and returns all parts, laid end to end along the dimension named above; an argument that names none is the same for every part. Nothing has to cross between parts.
All inputs are finite; a program needn't handle non-finite values.
Results may differ from a plain program's by a relative error of at most 0.013.
Values may be sent and summed in bfloat16 or wider, within the bound.
A program may use at most 64 MiB of HBM per device.

v0:
```python
import jax
import jax.numpy as jnp
from jax import lax
from jax.sharding import PartitionSpec as P

epsilon = 1e-05


def passed_along(value, axis, steps):
    count = lax.axis_size(axis)
    first, last = (max(0, -steps), min(count, count - steps))
    return lax.ppermute(value, axis, [(source, source + steps) for source in range(first, last)])


def local(
    activations, value_weight, gate_weight, conv_taps, conv_bias, norm_gain, norm_bias, out_weight
):
    tokens = activations[0]
    tok_rows = tokens.shape[0]
    kernel_len = conv_taps.shape[0]
    whole_value, whole_gate = (
        lax.all_gather(value_weight, "sp", axis=0, tiled=True),
        lax.all_gather(gate_weight, "sp", axis=0, tiled=True),
    )
    stacked = jnp.stack([whole_value, whole_gate], axis=0)
    both_rows = jnp.einsum(
        "td,kdc->ktc",
        tokens,
        lax.all_gather(stacked, "dp", axis=2, tiled=True),
        preferred_element_type=jnp.float32,
    )
    value_rows = both_rows[0]
    gate_rows = both_rows[1]
    value_half = value_rows.astype(jnp.bfloat16)
    gate_half = gate_rows.astype(jnp.bfloat16)
    gated_rows = (
        value_half.astype(jnp.float32) * jax.nn.sigmoid(gate_half.astype(jnp.float32))
    ).astype(jnp.bfloat16)
    prior = passed_along(gated_rows[tok_rows - (kernel_len - 1) :], "sp", 1)
    padded = jnp.concatenate([prior, gated_rows], axis=0).astype(jnp.float32)
    conv_sum = jnp.zeros(gated_rows.shape, jnp.float32) + conv_bias[None, :]
    for tap_index in range(kernel_len):
        conv_sum = (
            conv_sum + conv_taps[tap_index][None, :] * padded[tap_index : tap_index + tok_rows]
        )
    mean_row = jnp.mean(conv_sum, axis=-1, keepdims=True)
    centered = conv_sum - mean_row
    spread = jnp.mean(centered * centered, axis=-1, keepdims=True)
    normed = centered * lax.rsqrt(spread + epsilon) * norm_gain[None, :] + norm_bias[None, :]
    swished = jax.nn.silu(normed).astype(jnp.bfloat16)
    whole_output = lax.all_gather(out_weight, "sp", axis=0, tiled=True)
    result = jnp.dot(
        swished,
        lax.all_gather(whole_output, "dp", axis=1, tiled=True),
        preferred_element_type=jnp.float32,
    )
    return result.astype(jnp.bfloat16)[None]


def solution(mesh):
    in_specs = (
        P(("grp", "dp"), "sp", None),
        P("sp", "dp"),
        P("sp", "dp"),
        P(),
        P(),
        P(),
        P(),
        P("sp", "dp"),
    )
    out_specs = P(("grp", "dp"), "sp", None)
    return jax.shard_map(local, mesh=mesh, in_specs=in_specs, out_specs=out_specs, check_vma=False)
```

profile of v0, /device:TPU:0, one launch (start us, length us, event | category | flops | bytes accessed | tf_op | source)
XLA Modules:
  0.0 207.2 jit_solution(12494679978274099827)
XLA Ops:
  6.5 0.7 all-gather.6.cloned.1.call-update
  7.3 0.0 all-gather.8.cloned.1.call-start
  7.3 0.7 all-gather.8.cloned.1.call-update
  8.0 0.0 all-gather.12.cloned.1.call-start
  8.1 0.7 all-gather.12.cloned.1.call-update
  8.7 0.0 all-gather.10.cloned.1.call-start
  8.8 30.9 %all-gather.6.cloned.1.call-done = bf16[2048,256]{1,0:T(8,128)(2,1)} async-done(((bf16[512,256]{1,0:T(8,128)(2,1)}), bf16[2048,256]{1,0:T(8,128)(2,1)}) %all-gather.6.cloned.1.call-update) | async-done | bytes 1048592 | tf_op jit(solution)/shard_map/all_gather | solution.py:22
  39.6 29.0 %all-gather.8.cloned.1.call-done = bf16[2048,256]{1,0:T(8,128)(2,1)} async-done(((bf16[512,256]{1,0:T(8,128)(2,1)}), bf16[2048,256]{1,0:T(8,128)(2,1)}) %all-gather.8.cloned.1.call-update) | async-done | bytes 1048592 | tf_op jit(solution)/shard_map/all_gather | solution.py:23
  68.6 3.1 %pad_maximum_fusion = bf16[2,2048,256]{2,1,0:T(8,128)(2,1)} fusion(bf16[1,2048,256]{2,1,0:T(8,128)(2,1)} %bitcast.50, bf16[1,2048,256]{2,1,0:T(8,128)(2,1)} %bitcast.49), kind=kLoop, calls=%fused_computation.64 | loop fusion | flops 1048576 | bytes 4194304 | tf_op jit(solution)/shard_map/stack | solution.py:25
  71.7 0.0 all-gather.10.cloned.1.call-update
  71.7 0.0 all-gather.14.cloned.1.call-start
  71.7 25.8 %all-gather.12.cloned.1.call-done = bf16[1024,512]{1,0:T(8,128)(2,1)} async-done(((bf16[256,512]{1,0:T(8,128)(2,1)}), bf16[1024,512]{1,0:T(8,128)(2,1)}) %all-gather.12.cloned.1.call-update) | async-done | bytes 1048592 | tf_op jit(solution)/shard_map/all_gather | solution.py:51
  97.6 0.0 all-gather.14.cloned.1.call-update
  97.6 0.0 copy-done.2
  97.6 0.1 fusion.44
  97.7 60.0 %all-gather.10.cloned.1.call-done = bf16[2,2048,1024]{2,1,0:T(8,128)(2,1)} async-done(((bf16[2,2048,256]{2,1,0:T(8,128)(2,1)}), bf16[2,2048,1024]{2,1,0:T(8,128)(2,1)}) %all-gather.10.cloned.1.call-update) | async-done | bytes 8388624 | tf_op jit(solution)/shard_map/all_gather | solution.py:29
  157.8 0.0 copy-done
  157.8 8.1 %convert_bitcast_fusion = bf16[2,512,1024]{2,1,0:T(8,128)(2,1)S(1)} fusion(bf16[2,2048,1024]{2,1,0:T(8,128)(2,1)} %all-gather.10.cloned.1.call-done, bf16[1,512,2048]{2,1,0:T(8,128)(2,1)S(1)} %copy-done), kind=kOutput, calls=%fused_computation.68 | convolution fusion | flops 4296015872 | bytes 12582912 | tf_op jit(solution)/shard_map/td,kdc->ktc/dot_general | solution.py:26
  165.8 0.6 multiply_convert_fusion
  166.5 3.4 %collective-permute-start = (bf16[30,1024]{1,0:T(8,128)(2,1)S(1)}, bf16[30,1024]{1,0:T(8,128)(2,1)S(1)}, u32[]{:S(2)}, u32[]{:S(2)}) collective-permute-start(bf16[30,1024]{1,0:T(8,128)(2,1)S(1)} %slice_bitcast_fusion), channel_id=1, source_target_pairs={{0,4},{4,8},{8,12},{1,5},{5,9},{9,13},{2,6},{6,10},{10,14},{3,7},{... | collective-permute-start | bytes 184328 | tf_op jit(solution)/shard_map/ppermute | solution.py:12
  169.9 0.6 fusion.48
  170.5 0.0 copy-start.3
  170.5 1.3 collective-permute-done
  171.8 0.3 maximum_convert_fusion
  172.1 9.8 %fusion.42 = (f32[512]{0:T(512)S(1)}, f32[512,1024]{1,0:T(8,128)S(1)}) fusion(f32[542,1024]{1,0:T(8,128)S(1)} %maximum_convert_fusion, f32[1024]{0:T(1024)S(1)} %bitcast.61, f32[1024]{0:T(1024)S(1)} %bitcast.62, f32[1024]{0:T(1024)S(1)} %bitcast.64, f32[1024]{0:T(1024)S(1)} %bitcast.65, f32[1024]{0:T(1024)S(1)} %bitcast.66, f32[1024]{0:T(1024)S(1)} %bitcast.67, ...), kind=kLoop, calls=%fused_computation.81 | loop fusion | flops 33029632 | bytes 67241984 | tf_op jit(solution)/shard_map/reduce_sum | solution.py:46
  181.9 0.0 copy-start.4
  181.9 0.0 copy-start.5
  182.0 1.3 copy-done.1
  183.3 0.3 multiply_reduce_fusion
  183.6 10.0 %all-gather.14.cloned.1.call-done = bf16[1024,2048]{1,0:T(8,128)(2,1)} async-done(((bf16[1024,512]{1,0:T(8,128)(2,1)}), bf16[1024,2048]{1,0:T(8,128)(2,1)}) %all-gather.14.cloned.1.call-update) | async-done | bytes 4194320 | tf_op jit(solution)/shard_map/all_gather | solution.py:54
  193.7 0.0 copy-done.5
  193.7 7.0 %fusion = bf16[1,512,2048]{2,1,0:T(8,128)(2,1)} fusion(bf16[1024,2048]{1,0:T(8,128)(2,1)} %all-gather.14.cloned.1.call-done, f32[512,1024]{1,0:T(8,128)} %copy-done.1, f32[1024]{0:T(1024)S(1)} %copy-done.4, f32[1024]{0:T(1024)S(1)} %copy-done.5, f32[512]{0:T(512)S(1)} %add_rsqrt_fusion, f32[512]{0:T(512)S(1)} %broadcast_multiply_fusion), kind=kOutput, calls=%fused_computation.1 | convolution fusion | flops 2153250816 | bytes 8400896 | tf_op jit(solution)/shard_map/dot_general | solution.py:52
  (10 shorter events, 0.1 us)
Async XLA Ops:
  6.5 151.2 %copy-start = (bf16[1,512,2048]{2,1,0:T(8,128)(2,1)S(1)}, bf16[1,512,2048]{2,1,0:T(8,128)(2,1)}, u32[]{:S(2)}) copy-start(bf16[1,512,2048]{2,1,0:T(8,128)(2,1)} %param.8) | copy-start | bytes 6291460
  6.5 33.1 %all-gather.6.cloned.1.call-start = ((), (), s32[]{:S(2)}) async-start(), calls=%async_computation | async-start | bytes 1310720 | tf_op jit(solution)/shard_map/all_gather | solution.py:22
  7.3 61.3 %all-gather.8.cloned.1.call-start = ((), (), s32[]{:S(2)}) async-start(), calls=%async_computation.1 | async-start | bytes 1310720 | tf_op jit(solution)/shard_map/all_gather | solution.py:23
  8.0 89.6 %all-gather.12.cloned.1.call-start = ((), (), s32[]{:S(2)}) async-start(), calls=%async_computation.3 | async-start | bytes 1310720 | tf_op jit(solution)/shard_map/all_gather | solution.py:51
  8.7 149.0 %all-gather.10.cloned.1.call-start = ((), (), s32[]{:S(2)}) async-start(), calls=%async_computation.2 | async-start | bytes 10485760 | tf_op jit(solution)/shard_map/all_gather | solution.py:29
  71.7 25.9 %copy-start.2 = (f32[31,1024]{1,0:T(8,128)S(1)}, f32[31,1024]{1,0:T(8,128)}, u32[]{:S(2)}) copy-start(f32[31,1024]{1,0:T(8,128)} %param.11) | copy-start | bytes 380932
  71.7 122.0 %all-gather.14.cloned.1.call-start = ((), (), s32[]{:S(2)}) async-start(), calls=%async_computation.4 | async-start | bytes 5242880 | tf_op jit(solution)/shard_map/all_gather | solution.py:54
  166.5 5.3 %collective-permute-start = (bf16[30,1024]{1,0:T(8,128)(2,1)S(1)}, bf16[30,1024]{1,0:T(8,128)(2,1)S(1)}, u32[]{:S(2)}, u32[]{:S(2)}) collective-permute-start(bf16[30,1024]{1,0:T(8,128)(2,1)S(1)} %slice_bitcast_fusion), channel_id=1, source_target_pairs={{0,4},{4,8},{8,12},{1,5},{5,9},{9,13},{2,6},{6,10},{10,14},{3,7},{... | collective-permute-start | bytes 184328 | tf_op jit(solution)/shard_map/ppermute | solution.py:12
  170.5 1.6 copy-start.3
  181.9 1.3 copy-start.1
  181.9 11.7 %copy-start.4 = (f32[1024]{0:T(1024)S(1)}, f32[1024]{0:T(1024)}, u32[]{:S(2)}) copy-start(f32[1024]{0:T(1024)} %param.14) | copy-start | bytes 12292
  181.9 11.7 %copy-start.5 = (f32[1024]{0:T(1024)S(1)}, f32[1024]{0:T(1024)}, u32[]{:S(2)}) copy-start(f32[1024]{0:T(1024)} %param.13) | copy-start | bytes 12292
Sparse Core Ops, SparseCore 0:
  8.9 30.6 all-gather.5
  41.2 27.3 all-gather.7
  70.2 27.3 all-gather.11
  99.0 58.7 all-gather.9
  159.2 34.4 all-gather.13
where the time goes:
time: 207 us
  waiting for transfers between devices  159 us (77%)
  matrix products  15 us (7%)
  other arithmetic  14.7 us (7%)
  between operations  13.3 us (6%)
  starting transfers between devices  3.55 us (2%)
    all_gather x1, waiting for transfers between devices, local(): lax.all_gather(stacked, 'dp', axis=2, tiled=True)  60 us
    all_gather x1, waiting for transfers between devices, local(): lax.all_gather(value_weight, 'sp', axis=0, tiled=True)  30.9 us
    all_gather x1, waiting for transfers between devices, local(): lax.all_gather(gate_weight, 'sp', axis=0, tiled=True)  29 us
    all_gather x1, waiting for transfers between devices, local(): whole_output = lax.all_gather(out_weight, 'sp', axis=0, tiled=True)  25.8 us
    all_gather x1, waiting for transfers between devices, local(): lax.all_gather(whole_output, 'dp', axis=1, tiled=True)  10 us
    reduce_sum x1, other arithmetic, local(): mean_row = jnp.mean(conv_sum, axis=-1, keepdims=True)  9.83 us
    dot_general x1, matrix products, local(): jnp.einsum('td,kdc->ktc', tokens, lax.all_gather(stacked, 'dp', axis=2, t...  8.06 us
    dot_general x1, matrix products, local(): jnp.dot(swished, lax.all_gather(whole_output, 'dp', axis=1, tiled=True),...  6.96 us
  transfers between devices with their start and end apart: 6, of which 6 were waited for; matrix products, arithmetic and copies ran while one was open for 11% of the time, Pallas kernels for 0%

commit v1 on v0

--- a/solution.py
+++ b/solution.py
@@ -4,6 +4,11 @@
 from jax.sharding import PartitionSpec as P
 
 epsilon = 1e-05
+
+
+def gather_blocks(shard, axis, along):
+    pieces = lax.all_gather(shard, axis)
+    return jnp.concatenate(pieces, axis=along)
 
 
 def passed_along(value, axis, steps):
@@ -50,9 +55,7 @@
     swished = jax.nn.silu(normed).astype(jnp.bfloat16)
     whole_output = lax.all_gather(out_weight, "sp", axis=0, tiled=True)
     result = jnp.dot(
-        swished,
-        lax.all_gather(whole_output, "dp", axis=1, tiled=True),
-        preferred_element_type=jnp.float32,
+        swished, gather_blocks(whole_output, "dp", 1), preferred_element_type=jnp.float32
     )
     return result.astype(jnp.bfloat16)[None]
 

time: 207 us -> 229 us (1.11)
  waiting for transfers between devices: 159 us -> 178 us
  local copies, waits for them, and re-layouts: 1.44 us -> 7.62 us
  matrix products: 15 us -> 12.2 us
    all_gather x1, waiting for transfers between devices: 10 us -> 31.2 us  [gather_blocks(): pieces = lax.all_gather(shard, axis)]
    reshape x0 -> x1, local copies, waits for them, and re-layouts: none -> 6.3 us  [gather_blocks(): return jnp.concatenate(pieces, axis=along)]
    all_gather x1, waiting for transfers between devices: 60 us -> 54.5 us  [local(): lax.all_gather(stacked, 'dp', axis=2, tiled=True)]
    all_gather x1, waiting for transfers between devices: 25.8 us -> 30.9 us  [local(): whole_output = lax.all_gather(out_weight, 'sp', axis=0, tiled=True)]
    dot_general x1, matrix products: 6.96 us -> 4.16 us  [local(): jnp.dot(swished, gather_blocks(whole_output, 'dp', 1), preferred_element_...]
  transfers between devices with their start and end apart: 6 -> 6, of which waited for: 6 -> 6; matrix products, arithmetic and copies ran while one was open for 11% -> 4% of each run, Pallas kernels for 0% -> 0%
where the time goes in v1:
time: 229 us
  waiting for transfers between devices  178 us (78%)
  other arithmetic  14.6 us (6%)
  between operations  13.3 us (6%)
  matrix products  12.2 us (5%)
  local copies, waits for them, and re-layouts  7.62 us (3%)
  starting transfers between devices  3.55 us (2%)
    all_gather x1, waiting for transfers between devices, local(): lax.all_gather(stacked, 'dp', axis=2, tiled=True)  54.5 us
    all_gather x1, waiting for transfers between devices, gather_blocks(): pieces = lax.all_gather(shard, axis)  31.2 us
    all_gather x1, waiting for transfers between devices, local(): whole_output = lax.all_gather(out_weight, 'sp', axis=0, tiled=True)  30.9 us
    all_gather x1, waiting for transfers between devices, local(): lax.all_gather(gate_weight, 'sp', axis=0, tiled=True)  29 us
    all_gather x1, waiting for transfers between devices, local(): lax.all_gather(value_weight, 'sp', axis=0, tiled=True)  28.9 us
    reduce_sum x1, other arithmetic, local(): mean_row = jnp.mean(conv_sum, axis=-1, keepdims=True)  9.72 us
    dot_general x1, matrix products, local(): jnp.einsum('td,kdc->ktc', tokens, lax.all_gather(stacked, 'dp', axis=2, t...  8.07 us
    reshape x1, local copies, waits for them, and re-layouts, gather_blocks(): return jnp.concatenate(pieces, axis=along)  6.3 us
  transfers between devices with their start and end apart: 6, of which 6 were waited for; matrix products, arithmetic and copies ran while one was open for 4% of the time, Pallas kernels for 0%

profile of v1, /device:TPU:0, one launch (start us, length us, event | category | flops | bytes accessed | tf_op | source)
XLA Modules:
  0.0 229.1 jit_solution(6985236189080519574)
XLA Ops:
  6.5 0.7 all-gather.13.cloned.1.call-update
  7.3 0.0 all-gather.7.cloned.1.call-start
  7.3 0.7 all-gather.7.cloned.1.call-update
  8.0 0.0 all-gather.9.cloned.1.call-start
  8.1 0.7 all-gather.9.cloned.1.call-update
  8.7 0.0 all-gather.15.cloned.1.call-start
  8.8 30.9 %all-gather.13.cloned.1.call-done = bf16[1024,512]{1,0:T(8,128)(2,1)} async-done(((bf16[256,512]{1,0:T(8,128)(2,1)}), bf16[1024,512]{1,0:T(8,128)(2,1)}) %all-gather.13.cloned.1.call-update) | async-done | bytes 1048592 | tf_op jit(solution)/shard_map/all_gather | solution.py:56
  39.6 0.0 all-gather.15.cloned.1.call-update
  39.7 0.0 all-gather.11.cloned.1.call-start
  39.7 28.9 %all-gather.7.cloned.1.call-done = bf16[2048,256]{1,0:T(8,128)(2,1)} async-done(((bf16[512,256]{1,0:T(8,128)(2,1)}), bf16[2048,256]{1,0:T(8,128)(2,1)}) %all-gather.7.cloned.1.call-update) | async-done | bytes 1048592 | tf_op jit(solution)/shard_map/all_gather | solution.py:27
  68.6 29.0 %all-gather.9.cloned.1.call-done = bf16[2048,256]{1,0:T(8,128)(2,1)} async-done(((bf16[512,256]{1,0:T(8,128)(2,1)}), bf16[2048,256]{1,0:T(8,128)(2,1)}) %all-gather.9.cloned.1.call-update) | async-done | bytes 1048592 | tf_op jit(solution)/shard_map/all_gather | solution.py:28
  97.6 3.1 %pad_maximum_fusion = bf16[2,2048,256]{2,1,0:T(8,128)(2,1)} fusion(bf16[1,2048,256]{2,1,0:T(8,128)(2,1)} %bitcast.56, bf16[1,2048,256]{2,1,0:T(8,128)(2,1)} %bitcast.55), kind=kLoop, calls=%fused_computation.64 | loop fusion | flops 1048576 | bytes 4194304 | tf_op jit(solution)/shard_map/stack | solution.py:30
  100.6 0.0 all-gather.11.cloned.1.call-update
  100.6 0.9 copy-done.2
  101.6 0.1 fusion.44
  101.6 31.2 %all-gather.15.cloned.1.call-done = bf16[4096,512]{1,0:T(8,128)(2,1)} async-done(((bf16[1024,512]{1,0:T(8,128)(2,1)}), bf16[4096,512]{1,0:T(8,128)(2,1)}) %all-gather.15.cloned.1.call-update) | async-done | bytes 4194320 | tf_op jit(solution)/shard_map/all_gather | solution.py:10
  132.8 6.3 %copy.9 = bf16[1024,4,512]{0,2,1:T(8,128)(2,1)} copy(bf16[1024,4,512]{2,0,1:T(8,128)(2,1)} %bitcast.54) | data formatting | bytes 8388608 | tf_op jit(solution)/shard_map/reshape | solution.py:11
  139.1 54.5 %all-gather.11.cloned.1.call-done = bf16[2,2048,1024]{2,1,0:T(8,128)(2,1)} async-done(((bf16[2,2048,256]{2,1,0:T(8,128)(2,1)}), bf16[2,2048,1024]{2,1,0:T(8,128)(2,1)}) %all-gather.11.cloned.1.call-update) | async-done | bytes 8388624 | tf_op jit(solution)/shard_map/all_gather | solution.py:34
  193.7 8.1 %convert_bitcast_fusion = bf16[2,512,1024]{2,1,0:T(8,128)(2,1)S(1)} fusion(bf16[2,2048,1024]{2,1,0:T(8,128)(2,1)} %all-gather.11.cloned.1.call-done, bf16[1,512,2048]{2,1,0:T(8,128)(2,1)S(1)} %copy-done), kind=kOutput, calls=%fused_computation.68 | convolution fusion | flops 4296015872 | bytes 12582912 | tf_op jit(solution)/shard_map/td,kdc->ktc/dot_general | solution.py:31
  201.7 0.6 multiply_convert_fusion
  202.4 3.4 %collective-permute-start = (bf16[30,1024]{1,0:T(8,128)(2,1)S(1)}, bf16[30,1024]{1,0:T(8,128)(2,1)S(1)}, u32[]{:S(2)}, u32[]{:S(2)}) collective-permute-start(bf16[30,1024]{1,0:T(8,128)(2,1)S(1)} %slice_bitcast_fusion), channel_id=1, source_target_pairs={{0,4},{4,8},{8,12},{1,5},{5,9},{9,13},{2,6},{6,10},{10,14},{3,7},{... | collective-permute-start | bytes 184328 | tf_op jit(solution)/shard_map/ppermute | solution.py:17
  205.8 0.6 fusion.48
  206.4 0.0 copy-start.3
  206.4 1.3 collective-permute-done
  207.7 0.3 maximum_convert_fusion
  208.0 9.7 %fusion.42 = (f32[512]{0:T(512)S(1)}, f32[512,1024]{1,0:T(8,128)S(1)}) fusion(f32[542,1024]{1,0:T(8,128)S(1)} %maximum_convert_fusion, f32[1024]{0:T(1024)S(1)} %bitcast.67, f32[1024]{0:T(1024)S(1)} %bitcast.68, f32[1024]{0:T(1024)S(1)} %bitcast.70, f32[1024]{0:T(1024)S(1)} %bitcast.71, f32[1024]{0:T(1024)S(1)} %bitcast.72, f32[1024]{0:T(1024)S(1)} %bitcast.73, ...), kind=kLoop, calls=%fused_computation.81 | loop fusion | flops 33029632 | bytes 67241984 | tf_op jit(solution)/shard_map/reduce_sum | solution.py:51
  217.7 0.0 copy-start.4
  217.7 0.0 copy-start.5
  217.8 0.3 multiply_reduce_fusion
  218.1 0.3 copy-done.4
  218.4 0.0 copy-done.5
  218.4 4.2 %fusion = bf16[1,512,2048]{2,1,0:T(8,128)(2,1)} fusion(bf16[1024,2048]{0,1:T(8,128)(2,1)S(1)} %bitcast.53, f32[512,1024]{1,0:T(8,128)S(1)} %get-tuple-element.6, f32[1024]{0:T(1024)S(1)} %copy-done.4, f32[1024]{0:T(1024)S(1)} %copy-done.5, f32[512]{0:T(512)S(1)} %add_rsqrt_fusion, f32[512]{0:T(512)S(1)} %broadcast_multiply_fusion), kind=kOutput, calls=%fused_computation.1 | convolution fusion | flops 2153250816 | bytes 8400896 | tf_op jit(solution)/shard_map/dot_general | solution.py:57
  (11 shorter events, 0.1 us)
Async XLA Ops:
  6.5 187.1 %copy-start = (bf16[1,512,2048]{2,1,0:T(8,128)(2,1)S(1)}, bf16[1,512,2048]{2,1,0:T(8,128)(2,1)}, u32[]{:S(2)}) copy-start(bf16[1,512,2048]{2,1,0:T(8,128)(2,1)} %param.8) | copy-start | bytes 6291460
  6.5 33.1 %all-gather.13.cloned.1.call-start = ((), (), s32[]{:S(2)}) async-start(), calls=%async_computation.3 | async-start | bytes 1310720 | tf_op jit(solution)/shard_map/all_gather | solution.py:56
  7.3 61.3 %all-gather.7.cloned.1.call-start = ((), (), s32[]{:S(2)}) async-start(), calls=%async_computation | async-start | bytes 1310720 | tf_op jit(solution)/shard_map/all_gather | solution.py:27
  8.0 89.6 %all-gather.9.cloned.1.call-start = ((), (), s32[]{:S(2)}) async-start(), calls=%async_computation.1 | async-start | bytes 1310720 | tf_op jit(solution)/shard_map/all_gather | solution.py:28
  8.7 124.1 %all-gather.15.cloned.1.call-start = ((), (), s32[]{:S(2)}) async-start(), calls=%async_computation.4 | async-start | bytes 5242880 | tf_op jit(solution)/shard_map/all_gather | solution.py:10
  39.7 154.0 %all-gather.11.cloned.1.call-start = ((), (), s32[]{:S(2)}) async-start(), calls=%async_computation.2 | async-start | bytes 10485760 | tf_op jit(solution)/shard_map/all_gather | solution.py:34
  100.6 0.9 copy-start.2
  202.4 5.3 %collective-permute-start = (bf16[30,1024]{1,0:T(8,128)(2,1)S(1)}, bf16[30,1024]{1,0:T(8,128)(2,1)S(1)}, u32[]{:S(2)}, u32[]{:S(2)}) collective-permute-start(bf16[30,1024]{1,0:T(8,128)(2,1)S(1)} %slice_bitcast_fusion), channel_id=1, source_target_pairs={{0,4},{4,8},{8,12},{1,5},{5,9},{9,13},{2,6},{6,10},{10,14},{3,7},{... | collective-permute-start | bytes 184328 | tf_op jit(solution)/shard_map/ppermute | solution.py:17
  206.4 1.6 copy-start.3
  208.0 10.1 %copy-start.1 = (bf16[1024,4,512]{0,2,1:T(8,128)(2,1)S(1)}, bf16[1024,4,512]{0,2,1:T(8,128)(2,1)}, u32[]{:S(2)}) copy-start(bf16[1024,4,512]{0,2,1:T(8,128)(2,1)} %copy.9) | copy-start | bytes 12582916
  217.7 0.7 copy-start.4
  217.7 0.7 copy-start.5
Sparse Core Ops, SparseCore 0:
  8.9 30.6 all-gather.12
  41.2 27.3 all-gather.6
  70.2 27.3 all-gather.8
  99.0 33.8 all-gather.14
  134.2 59.3 all-gather.10
